TPU v7x, 32 devices: a whole 2x2x4 slice. The times are simulated.
32 devices in a mesh: ep: 8 (over z, core), tp: 4 (over y, x).
Axes of the slice: x: 2, y: 2, z: 4, core: 2. Of those that a mesh axis runs over, the one named last changes fastest.
Arguments:
- query_maps: bfloat16 [2048, 4096], P('ep', 'tp'), may hold values from -40 to 40
- key_maps: bfloat16 [2048, 4096], P('ep', 'tp'), may hold values from -40 to 40
- value_rows: bfloat16 [2048, 4096], P('ep', 'tp'), may hold values from -6 to 6
- head_lambda: float32 [16], P('tp'), may hold values from 0.3 to 0.8
- head_gain: float32 [256], replicated, may hold values from 0.1 to 1.9
- out_weight: bfloat16 [4096, 2048], P('tp'), may hold values from -0.125 to 0.125
- expert_rows: bfloat16 [1024, 2048], P('ep'), may hold values from -6 to 6
- expert_gain: float32 [2048], replicated, may hold values from 0.1 to 1.9
- routes: int32 [1024, 2], P('ep'), may hold values from 0 to 7, all different within a row; in each aligned block of 128 rows (0 to 127, 128 to 255, ...) at most 48 rows name the same one
- route_weights: float32 [1024, 2], P('ep'), may hold values from 0.2 to 1
- gate_weight: bfloat16 [8, 2048, 4096], P('ep', None, 'tp'), may hold values from -0.125 to 0.125
- up_weight: bfloat16 [8, 2048, 4096], P('ep', None, 'tp'), may hold values from -0.125 to 0.125
- down_weight: bfloat16 [8, 4096, 2048], P('ep', 'tp'), may hold values from -0.125 to 0.125
Outputs:
- mixed: bfloat16 [2048, 2048], P('ep', 'tp')
- expert_out: bfloat16 [1024, 2048], P('ep', 'tp')
Inputs may be any that keep to these rules, and one draw needn't show every extreme that they name: `routes`: within the rows of one device (aligned blocks of 128 rows) no expert is named more than 48 times, and the 2 experts of a row differ.
All inputs are finite; a program needn't handle non-finite values.
Results may differ from a plain program's by a relative error of at most 0.018.
Values may be sent and summed in bfloat16 or wider, within the bound.
A program may use at most 128 MiB of HBM per device.

v0:
```python
import jax
import jax.numpy as jnp
from jax import lax
from jax.sharding import PartitionSpec as P

norm_eps = 1e-06
rope_base = 10000.0


def rope_turn(inputs, positions):
    half_dim = inputs.shape[-1] // 2
    inverse = rope_base ** (-2.0 * jnp.arange(half_dim, dtype=jnp.float32) / inputs.shape[-1])
    angles = positions.astype(jnp.float32)[:, None] * inverse[None, :]
    cos_table = jnp.cos(angles)[:, None, None, :]
    sin_table = jnp.sin(angles)[:, None, None, :]
    first_half = inputs[..., :half_dim]
    second_half = inputs[..., half_dim:]
    return jnp.concatenate(
        [
            first_half * cos_table - second_half * sin_table,
            second_half * cos_table + first_half * sin_table,
        ],
        axis=-1,
    )


def mixer_half(query_maps, key_maps, value_rows, head_lambda, head_gain, out_weight):
    row_count = query_maps.shape[0]
    head_count = head_lambda.shape[0]
    head_dim = query_maps.shape[1] // (2 * head_count)
    value_dim = value_rows.shape[1] // head_count
    model_width = out_weight.shape[1]
    score_scale = head_dim ** (-0.5)
    offset = lax.axis_index("ep") * row_count
    positions = offset + jnp.arange(row_count, dtype=jnp.int32)
    last_row = offset + row_count - 1
    rotated_q = rope_turn(
        query_maps.astype(jnp.float32).reshape(row_count, head_count, 2, head_dim), positions
    ).astype(jnp.bfloat16)
    rotated_k = rope_turn(
        key_maps.astype(jnp.float32).reshape(row_count, head_count, 2, head_dim), positions
    ).astype(jnp.bfloat16)
    rotated_k = rotated_k.reshape(row_count, head_count * 2 * head_dim)
    initial = (
        jnp.full((head_count, 2, row_count), -1e30, jnp.float32),
        jnp.zeros((head_count, 2, row_count), jnp.float32),
        jnp.zeros((head_count, 2, row_count, value_dim), jnp.float32),
    )
    piece_k = lax.all_gather(rotated_k, "ep", axis=0, tiled=True)
    piece_v = lax.all_gather(value_rows, "ep", axis=0, tiled=True)
    piece_len = piece_k.shape[0]
    block_size = 1024

    def attend(state):

        def fold_step(inner, block_index):
            block_start = block_index * block_size
            block_k = lax.dynamic_slice_in_dim(piece_k, block_start, block_size, 0).reshape(
                block_size, head_count, 2, head_dim
            )
            block_v = lax.dynamic_slice_in_dim(piece_v, block_start, block_size, 0).reshape(
                block_size, head_count, value_dim
            )
            scores = (
                jnp.einsum(
                    "qhmd,khmd->hmqk", rotated_q, block_k, preferred_element_type=jnp.float32
                )
                * score_scale
            )
            key_pos = block_start + jnp.arange(block_size, dtype=jnp.int32)
            causal = key_pos[None, :] <= positions[:, None]
            masked = jnp.where(causal, scores, -1e30)
            run_max, run_sum, run_acc = inner
            new_max = jnp.maximum(run_max, jnp.max(masked, axis=-1))
            expd = jnp.where(causal, jnp.exp(masked - new_max[..., None]), 0.0)
            rescale = jnp.exp(run_max - new_max)
            new_sum = run_sum * rescale + jnp.sum(expd, axis=-1)
            new_acc = run_acc * rescale[..., None] + jnp.einsum(
                "hmqk,khe->hmqe",
                expd.astype(jnp.bfloat16),
                block_v,
                preferred_element_type=jnp.float32,
            )
            return ((new_max, new_sum, new_acc), None)

        result, _ = lax.scan(fold_step, state, jnp.arange(piece_len // block_size, dtype=jnp.int32))
        return result

    def skip_piece(state):
        return state

    run_max, run_sum, run_acc = lax.cond(jnp.int32(0) <= last_row, attend, skip_piece, initial)
    first_map = run_acc[:, 0] / run_sum[:, 0][..., None]
    second_map = run_acc[:, 1] / run_sum[:, 1][..., None]
    difference = first_map - head_lambda[:, None, None] * second_map
    head_out = (
        difference
        * lax.rsqrt(jnp.mean(difference * difference, axis=-1, keepdims=True) + norm_eps)
        * head_gain
    ).astype(jnp.bfloat16)
    partial_value = jnp.einsum(
        "hqe,hed->qd",
        head_out,
        out_weight.reshape(head_count, value_dim, model_width),
        preferred_element_type=jnp.float32,
    )
    return lax.psum_scatter(
        partial_value.astype(jnp.bfloat16), "tp", scatter_dimension=1, tiled=True
    )


def expert_half(
    expert_rows, expert_gain, routes, route_weights, gate_weight, up_weight, down_weight
):
    ep_count = lax.axis_size("ep")
    tp_count = lax.axis_size("tp")
    row_count, model_width = expert_rows.shape
    pick_count = routes.shape[1]
    capacity = 3 * row_count * pick_count // (2 * ep_count)
    column_count = model_width // tp_count
    inputs = expert_rows.astype(jnp.float32)
    normed = (
        inputs
        * lax.rsqrt(jnp.mean(inputs * inputs, axis=-1, keepdims=True) + norm_eps)
        * expert_gain
    ).astype(jnp.bfloat16)
    expert_ids = routes.reshape(-1)
    one_hot = (expert_ids[:, None] == jnp.arange(ep_count, dtype=jnp.int32)[None, :]).astype(
        jnp.int32
    )
    slot_index = jnp.sum((jnp.cumsum(one_hot, axis=0) - one_hot) * one_hot, axis=1)
    source_row = jnp.arange(row_count * pick_count, dtype=jnp.int32) // pick_count
    empty = jnp.zeros((ep_count, capacity, normed.shape[1]), jnp.bfloat16)
    arrived = lax.all_to_all(
        empty.at[expert_ids, slot_index].set(normed[source_row]),
        "ep",
        split_axis=0,
        concat_axis=0,
        tiled=True,
    )
    slot_count = arrived.shape[1]
    flat_rows = arrived.reshape(ep_count * slot_count, model_width)
    gate_values = jnp.dot(flat_rows, gate_weight[0], preferred_element_type=jnp.float32)
    up_values = jnp.dot(flat_rows, up_weight[0], preferred_element_type=jnp.float32)
    hidden = (jax.nn.silu(gate_values) * up_values).astype(jnp.bfloat16)
    partial_value = jnp.dot(hidden, down_weight[0], preferred_element_type=jnp.float32).reshape(
        ep_count, slot_count, model_width
    )
    summed = lax.psum_scatter(
        partial_value.astype(jnp.bfloat16), "tp", scatter_dimension=2, tiled=True
    )
    returned = lax.all_to_all(summed, "ep", split_axis=0, concat_axis=0, tiled=True)
    picked = returned[expert_ids, slot_index].reshape(row_count, pick_count, column_count)
    combined = jnp.sum(route_weights[..., None] * picked.astype(jnp.float32), axis=1)
    return combined.astype(jnp.bfloat16)


def on_device(
    query_maps,
    key_maps,
    value_rows,
    head_lambda,
    head_gain,
    out_weight,
    expert_rows,
    expert_gain,
    routes,
    route_weights,
    gate_weight,
    up_weight,
    down_weight,
):
    mixed = mixer_half(query_maps, key_maps, value_rows, head_lambda, head_gain, out_weight)
    expert_out = expert_half(
        expert_rows, expert_gain, routes, route_weights, gate_weight, up_weight, down_weight
    )
    return (mixed, expert_out)


def solution(mesh):
    placed = (
        P("ep", "tp"),
        P("ep", "tp"),
        P("ep", "tp"),
        P("tp"),
        P(),
        P("tp", None),
        P("ep", None),
        P(),
        P("ep", None),
        P("ep", None),
        P("ep", None, "tp"),
        P("ep", None, "tp"),
        P("ep", "tp", None),
    )
    return jax.shard_map(
        on_device,
        mesh=mesh,
        in_specs=placed,
        out_specs=(P("ep", "tp"), P("ep", "tp")),
        check_vma=False,
    )
```

profile of v0, /device:TPU:0, one launch (start us, length us, event | category | flops | bytes accessed | tf_op | source)
XLA Modules:
  0.0 216.2 jit_solution(5732117956623233506)
XLA Ops:
  8.1 1.3 copy.21
  10.1 1.1 subtract_convert_fusion
  11.2 0.8 pad_maximum_fusion
  12.1 1.0 copy.23
  15.1 1.4 gather_fusion
  16.7 23.1 %scatter_fusion = bf16[8,48,2048]{2,1,0:T(8,128)(2,1)S(1)} fusion(bf16[8,48,2048]{2,1,0:T(8,128)(2,1)S(1)} %broadcast_in_dim.33, s32[256]{0:T(256)S(1)} %bitcast.103, bf16[256,2048]{1,0:T(8,128)(2,1)S(1)} %gather_fusion), kind=kCustom, calls=%fused_computation.2 | custom fusion | bytes 3147776 | tf_op jit(solution)/shard_map/scatter | solution.py:135
  39.8 63.6 %all_to_all.10 = bf16[8,48,2048]{2,1,0:T(8,128)(2,1)S(1)} all-to-all(bf16[8,48,2048]{2,1,0:T(8,128)(2,1)S(1)} %scatter_fusion), channel_id=1, replica_groups=mesh['ep'=8,'tp'=4] {'ep'}, dimensions={0} | all-to-all | bytes 3145728 | tf_op jit(solution)/shard_map/all_to_all | solution.py:134
  103.4 4.1 %fusion.18 = f32[384,1024]{1,0:T(8,128)S(1)} fusion(bf16[384,2048]{1,0:T(8,128)(2,1)S(1)} %bitcast.108, bf16[1,2048,1024]{2,1,0:T(8,128)(2,1)} %param.27), kind=kOutput, calls=%fused_computation.29 | convolution fusion | flops 1610612736 | bytes 7340032 | tf_op jit(solution)/shard_map/dot_general | solution.py:143
  107.6 2.0 multiply_convert_fusion
  109.8 3.0 %fusion.20 = bf16[8,48,2048]{2,1,0:T(8,128)(2,1)} fusion(bf16[8,48,1024]{2,1,0:T(8,128)(2,1)S(1)} %bitcast.113, bf16[1,1024,2048]{2,1,0:T(8,128)(2,1)S(1)} %copy-done.11), kind=kOutput, calls=%fused_computation.31 | convolution fusion | flops 1611399168 | bytes 6553600 | tf_op jit(solution)/shard_map/dot_general | solution.py:146
  113.1 18.7 %all-gather.5.cloned.1.call-done = bf16[2048,1024]{0,1:T(8,128)(2,1)} async-done(((bf16[256,1024]{0,1:T(8,128)(2,1)}), bf16[2048,1024]{0,1:T(8,128)(2,1)}) %all-gather.5.cloned.1.call-update) | async-done | bytes 4194320 | tf_op jit(solution)/shard_map/all_gather | solution.py:50
  131.8 40.5 %conditional.1 = (f32[4,2,256]{2,1,0:T(2,128)}, f32[4,2,256,256]{3,2,1,0:T(8,128)}) conditional(s32[]{:T(128)} %convert_element_type.56, () %tuple.20, (s32[]{:T(128)}, s32[256]{0:T(256)S(1)}, bf16[2048,1024]{0,1:T(8,128)(2,1)}, bf16[256,4,2,128]{0,3,2,1:T(8,128)(2,1)S(1)}, bf16[2048,1024]{0,1:T(8,128)(2,1)}) %tuple.21), branch_computations={%region_0.0_spmd, %region_1.6_spmd} | conditional | flops 1639722240 | bytes 78261616 | solution.py:92
  132.2 40.2 %while.14 = (s32[]{:T(128)}, f32[4,2,256]{2,1,0:T(2,128)S(1)}, f32[4,2,256]{2,1,0:T(2,128)}, f32[4,2,256,256]{3,2,1,0:T(8,128)}, s32[2]{0:T(128)S(1)}, /*index=5...) while((s32[]{:T(128)}, f32[4,2,256]{2,1,0:T(2,128)S(1)}, ...), condition=%wide.region_5.5_spmd.clone, body=%wide.region_2.4_spmd.clone.sunk | while | flops 1639721984 | bytes 77210856 | solution.py:86
  132.2 0.6 dynamic_slice.18
  133.4 2.9 %constant_dynamic-slice_fusion.3 = (bf16[1024,1024]{0,1:T(8,128)(2,1)S(1)}, bf16[1024,1024]{0,1:T(8,128)(2,1)S(1)}) fusion(bf16[2048,1024]{0,1:T(8,128)(2,1)} %get-tuple-element.247, s32[]{:T(128)S(6)} %select_n.109, bf16[2048,1024]{0,1:T(8,128)(2,1)} %get-tuple-element.245), kind=kLoop, calls=%fused_computation.19.clone.1 | loop fusion | bytes 8388612 | tf_op jit(solution)/shard_map/cond/branch_1_fun/while/body/eval_jaxpr/dynamic_slice | solution.py:61
  136.6 4.9 %fusion.62 = (f32[4,2,256]{2,1,0:T(2,128)S(1)}, f32[4,2,1024,256]{3,2,1,0:T(8,128)}) fusion(pred[256,1024]{0,1:T(8,128)(4,1)S(1)} %broadcast_compare_fusion.2, bf16[1024,4,2,128]{0,3,2,1:T(8,128)(2,1)S(1)} %bitcast.101, bf16[256,4,2,128]{3,0,2,1:T(8,128)(2,1)S(1)} %get-tuple-element.246), kind=kOutput, calls=%fused_computation.5.clone.1 | convolution fusion | flops 543160320 | bytes 11280384 | tf_op jit(solution)/shard_map/cond/branch_1_fun/while/body/eval_jaxpr/qhmd,khmd->hmqk/dot_general | solution.py:65
  141.5 4.6 %fusion.64 = f32[4,2,256]{2,1,0:T(2,128)S(1)} fusion(f32[4,2,1024,256]{3,2,1,0:T(8,128)} %get-tuple-element.209, f32[4,2,256]{2,1,0:T(2,128)S(1)} %fusion.63, pred[256,1024]{0,1:T(8,128)(4,1)S(1)} %broadcast_compare_fusion.2), kind=kLoop, calls=%fused_computation.7.clone.1 | loop fusion | flops 10483712 | bytes 8667136 | tf_op jit(solution)/shard_map/cond/branch_1_fun/while/body/eval_jaxpr/reduce_sum | solution.py:77
  146.1 0.6 fusion.65
  147.4 4.3 %fusion.66 = f32[4,2,256,256]{3,2,1,0:T(8,128)} fusion(f32[4,2,256,256]{3,2,1,0:T(8,128)} %get-tuple-element.229, bf16[1024,4,256,1]{0,2,3,1:T(8,128)(2,1)S(1)} %bitcast.102, f32[4,2,1024,256]{3,2,1,0:T(8,128)S(1)} %copy-done, f32[4,2,256]{2,1,0:T(2,128)S(1)} %fusion.63, pred[256,1024]{0,1:T(8,128)(4,1)S(1)} %broadcast_compare_fusion.2, ...), kind=kOutput, calls=%fused_computation.11.clone.1 | convolution fusion | flops 1085800448 | bytes 14958593 | tf_op jit(solution)/shard_map/cond/branch_1_fun/while/body/eval_jaxpr/hmqk,khe->hmqe/dot_general | solution.py:78
  152.9 2.7 %constant_dynamic-slice_fusion.3 = (bf16[1024,1024]{0,1:T(8,128)(2,1)S(1)}, bf16[1024,1024]{0,1:T(8,128)(2,1)S(1)}) fusion(bf16[2048,1024]{0,1:T(8,128)(2,1)} %get-tuple-element.247, s32[]{:T(128)S(6)} %select_n.109, bf16[2048,1024]{0,1:T(8,128)(2,1)} %get-tuple-element.245), kind=kLoop, calls=%fused_computation.19.clone.1 | loop fusion | bytes 8388612 | tf_op jit(solution)/shard_map/cond/branch_1_fun/while/body/eval_jaxpr/dynamic_slice | solution.py:61
  155.8 4.9 %fusion.62 = (f32[4,2,256]{2,1,0:T(2,128)S(1)}, f32[4,2,1024,256]{3,2,1,0:T(8,128)}) fusion(pred[256,1024]{0,1:T(8,128)(4,1)S(1)} %broadcast_compare_fusion.2, bf16[1024,4,2,128]{0,3,2,1:T(8,128)(2,1)S(1)} %bitcast.101, bf16[256,4,2,128]{3,0,2,1:T(8,128)(2,1)S(1)} %get-tuple-element.246), kind=kOutput, calls=%fused_computation.5.clone.1 | convolution fusion | flops 543160320 | bytes 11280384 | tf_op jit(solution)/shard_map/cond/branch_1_fun/while/body/eval_jaxpr/qhmd,khmd->hmqk/dot_general | solution.py:65
  160.7 4.6 %fusion.64 = f32[4,2,256]{2,1,0:T(2,128)S(1)} fusion(f32[4,2,1024,256]{3,2,1,0:T(8,128)} %get-tuple-element.209, f32[4,2,256]{2,1,0:T(2,128)S(1)} %fusion.63, pred[256,1024]{0,1:T(8,128)(4,1)S(1)} %broadcast_compare_fusion.2), kind=kLoop, calls=%fused_computation.7.clone.1 | loop fusion | flops 10483712 | bytes 8667136 | tf_op jit(solution)/shard_map/cond/branch_1_fun/while/body/eval_jaxpr/reduce_sum | solution.py:77
  165.3 1.5 fusion.65
  166.9 5.5 %fusion.66 = f32[4,2,256,256]{3,2,1,0:T(8,128)} fusion(f32[4,2,256,256]{3,2,1,0:T(8,128)} %get-tuple-element.229, bf16[1024,4,256,1]{0,2,3,1:T(8,128)(2,1)S(1)} %bitcast.102, f32[4,2,1024,256]{3,2,1,0:T(8,128)S(1)} %copy-done, f32[4,2,256]{2,1,0:T(2,128)S(1)} %fusion.63, pred[256,1024]{0,1:T(8,128)(4,1)S(1)} %broadcast_compare_fusion.2, ...), kind=kOutput, calls=%fused_computation.11.clone.1 | convolution fusion | flops 1085800448 | bytes 14958593 | tf_op jit(solution)/shard_map/cond/branch_1_fun/while/body/eval_jaxpr/hmqk,khe->hmqe/dot_general | solution.py:78
  172.4 0.8 fusion.40
  173.2 2.1 multiply_reduce_fusion
  175.3 4.5 %fusion.23 = bf16[256,2048]{1,0:T(8,128)(2,1)} fusion(bf16[4,256,2048]{2,1,0:T(8,128)(2,1)} %bitcast.112, f32[4,256,256]{2,1,0:T(8,128)S(1)} %get-tuple-element.129, f32[256]{0:T(256)S(1)} %copy-done.12, f32[4,256]{1,0:T(4,128)S(1)} %add_rsqrt_fusion), kind=kOutput, calls=%fused_computation.33 | convolution fusion | flops 1075052544 | bytes 6296576 | tf_op jit(solution)/shard_map/hqe,hed->qd/dot_general | solution.py:101
  179.8 4.8 %all-to-all-start.1 = ((bf16[8,48,512]{2,1,0:T(8,128)(2,1)}), bf16[8,48,512]{2,1,0:T(8,128)(2,1)S(1)}, u32[]{:S(2)}, u32[]{:S(2)}) async-start(bf16[8,48,512]{2,1,0:T(8,128)(2,1)} %reduce-scatter.5.cloned.1.call-done), calls=%async_computation.3 | async-start | bytes 786432 | tf_op jit(solution)/shard_map/all_to_all | solution.py:152
  184.7 12.4 %all-to-all-done.1 = bf16[8,48,512]{2,1,0:T(8,128)(2,1)S(1)} async-done(((bf16[8,48,512]{2,1,0:T(8,128)(2,1)}), bf16[8,48,512]{2,1,0:T(8,128)(2,1)S(1)}, u32[]{:S(2)}, u32[]{:S(2)}) %all-to-all-start.1) | async-done | bytes 393248 | tf_op jit(solution)/shard_map/all_to_all | solution.py:152
  197.1 2.1 gather_fusion.1
  199.5 1.4 multiply_reduce_fusion.1
  200.9 7.9 %reduce-scatter.3.cloned.1.call-done = bf16[256,512]{1,0:T(8,128)(2,1)} async-done(((bf16[256,2048]{1,0:T(8,128)(2,1)}), bf16[256,512]{1,0:T(8,128)(2,1)}) %reduce-scatter.3.cloned.1.call-update) | async-done | bytes 262160 | tf_op jit(solution)/shard_map/reduce_scatter | solution.py:107
  (82 shorter events, 5.9 us)
Async XLA Ops:
  8.0 1.5 copy-start.4
  8.0 105.1 %all-gather.3.cloned.1.call-start = ((), (), s32[]{:S(2)}) async-start(), calls=%async_computation.4 | async-start | bytes 4718592 | tf_op jit(solution)/shard_map/all_gather | solution.py:49
  10.1 2.0 copy-start.5
  11.2 2.0 copy-start.7
  11.2 3.4 %copy-start.1 = (bf16[128,2048]{1,0:T(8,128)(2,1)S(1)}, bf16[128,2048]{1,0:T(8,128)(2,1)}, u32[]{:S(2)}) copy-start(bf16[128,2048]{1,0:T(8,128)(2,1)} %param.23) | copy-start | bytes 1572868
  11.2 3.6 %copy-start.6 = (f32[2048]{0:T(1024)S(1)}, f32[2048]{0:T(1024)}, u32[]{:S(2)}) copy-start(f32[2048]{0:T(1024)} %param.24) | copy-start | bytes 24580
  12.1 119.7 %all-gather.5.cloned.1.call-start = ((), (), s32[]{:S(2)}) async-start(), calls=%async_computation.5 | async-start | bytes 4718592 | tf_op jit(solution)/shard_map/all_gather | solution.py:50
  13.2 166.6 %reduce-scatter.5.cloned.1.call-start = ((), (), s32[]{:S(2)}) async-start(), calls=%async_computation.7 | async-start | bytes 1966080 | tf_op jit(solution)/shard_map/reduce_scatter | solution.py:149
  103.4 4.1 %copy-start.10 = (bf16[1,2048,1024]{2,1,0:T(8,128)(2,1)S(1)}, bf16[1,2048,1024]{2,1,0:T(8,128)(2,1)}, u32[]{:S(2)}) copy-start(bf16[1,2048,1024]{2,1,0:T(8,128)(2,1)} %param.28) | copy-start | bytes 12582916
  107.6 2.2 %copy-start.11 = (bf16[1,1024,2048]{2,1,0:T(8,128)(2,1)S(1)}, bf16[1,1024,2048]{2,1,0:T(8,128)(2,1)}, u32[]{:S(2)}) copy-start(bf16[1,1024,2048]{2,1,0:T(8,128)(2,1)} %param.29) | copy-start | bytes 12582916
  109.8 3.2 %copy-start.2 = (bf16[256,4,2,64]{0,3,2,1:T(8,128)(2,1)S(1)}, bf16[256,4,2,64]{0,3,2,1:T(8,128)(2,1)}, u32[]{:S(2)}) copy-start(bf16[256,4,2,64]{0,3,2,1:T(8,128)(2,1)} %get-tuple-element.134) | copy-start | bytes 786436
  109.8 3.3 %copy-start.3 = (bf16[256,4,2,64]{0,3,2,1:T(8,128)(2,1)S(1)}, bf16[256,4,2,64]{0,3,2,1:T(8,128)(2,1)}, u32[]{:S(2)}) copy-start(bf16[256,4,2,64]{0,3,2,1:T(8,128)(2,1)} %get-tuple-element.135) | copy-start | bytes 786436
  112.8 96.1 %reduce-scatter.3.cloned.1.call-start = ((), (), s32[]{:S(2)}) async-start(), calls=%async_computation.6 | async-start | bytes 1310720 | tf_op jit(solution)/shard_map/reduce_scatter | solution.py:107
  131.8 41.3 %copy-start.9 = (f32[4]{0:T(128)S(1)}, f32[4]{0:T(128)}, u32[]{:S(2)}) copy-start(f32[4]{0:T(128)} %param.20) | copy-start | bytes 52
  141.5 5.9 %copy-start = (f32[4,2,1024,256]{3,2,1,0:T(8,128)S(1)}, f32[4,2,1024,256]{3,2,1,0:T(8,128)}, u32[]{:S(2)}) copy-start(f32[4,2,1024,256]{3,2,1,0:T(8,128)} %get-tuple-element.209) | copy-start | bytes 25165828 | tf_op jit(solution)/shard_map/cond/branch_1_fun/while
  160.7 6.2 %copy-start = (f32[4,2,1024,256]{3,2,1,0:T(8,128)S(1)}, f32[4,2,1024,256]{3,2,1,0:T(8,128)}, u32[]{:S(2)}) copy-start(f32[4,2,1024,256]{3,2,1,0:T(8,128)} %get-tuple-element.209) | copy-start | bytes 25165828 | tf_op jit(solution)/shard_map/cond/branch_1_fun/while
  172.3 2.9 %copy-start.12 = (f32[256]{0:T(256)S(1)}, f32[256]{0:T(256)}, u32[]{:S(2)}) copy-start(f32[256]{0:T(256)} %param.21) | copy-start | bytes 3076
  175.3 9.3 %copy-start.8 = (f32[128,2]{0,1:T(2,128)S(1)}, f32[128,2]{0,1:T(2,128)}, u32[]{:S(2)}) copy-start(f32[128,2]{0,1:T(2,128)} %param.26) | copy-start | bytes 3076
  179.8 17.3 %all-to-all-start.1 = ((bf16[8,48,512]{2,1,0:T(8,128)(2,1)}), bf16[8,48,512]{2,1,0:T(8,128)(2,1)S(1)}, u32[]{:S(2)}, u32[]{:S(2)}) async-start(bf16[8,48,512]{2,1,0:T(8,128)(2,1)} %reduce-scatter.5.cloned.1.call-done), calls=%async_computation.3 | async-start | bytes 786432 | tf_op jit(solution)/shard_map/all_to_all | solution.py:152
Sparse Core Ops, SparseCore 0:
  12.2 66.4 all-gather.2
  80.3 51.4 all-gather.4
Sparse Core Ops, SparseCore 1:
  112.8 29.0 reduce-scatter.4
  179.9 28.9 reduce-scatter.2
where the time goes:
time: 217 us; the launch traced here: 216 us
  blocking collectives  63.6 us (29%)
  waiting for transfers between devices  39.2 us (18%)
  local copies, waits for them, and re-layouts  39.1 us (18%)
  matrix products  33.2 us (15%)
  other arithmetic  18.9 us (9%)
  between operations  15.8 us (7%)
  starting transfers between devices  5.1 us (2%)
    all_to_all x1, blocking collectives, expert_half(): lax.all_to_all(empty.at[expert_ids, slot_index].set(normed[source_row]),...  63.6 us
    scatter x1, local copies, waits for them, and re-layouts, expert_half(): empty.at[expert_ids, slot_index].set(normed[source_row])  23.1 us
    all_gather x1, waiting for transfers between devices, mixer_half(): piece_v = lax.all_gather(value_rows, 'ep', axis=0, tiled=True)  18.7 us
    all_to_all x1, waiting for transfers between devices, expert_half(): lax.all_to_all(summed, 'ep', split_axis=0, concat_axis=0, tiled=True)  12.4 us
    dot_general x2, matrix products, fold_step(): jnp.einsum('qhmd,khmd->hmqk', rotated_q, block_k, preferred_element_type=...  9.86 us
    dot_general x2, matrix products, fold_step(): jnp.einsum('hmqk,khe->hmqe', expd.astype(jnp.bfloat16), block_v, preferre...  9.77 us
    reduce_sum x2, other arithmetic, fold_step(): new_sum = run_sum * rescale + jnp.sum(expd, axis=-1)  9.24 us
    reduce_scatter x1, waiting for transfers between devices, mixer_half(): lax.psum_scatter(partial_value.astype(jnp.bfloat16), 'tp', scatter_dimens...  7.92 us
  transfers between devices with their start and end apart: 5, of which 3 were waited for; matrix products, arithmetic and copies ran while one was open for 40% of the time, Pallas kernels for 0%

commit v1 on v0

--- a/solution.py
+++ b/solution.py
@@ -1,6 +1,10 @@
+import functools
+
 import jax
 import jax.numpy as jnp
 from jax import lax
+from jax.experimental import pallas as pl
+from jax.experimental.pallas import tpu as pltpu
 from jax.sharding import PartitionSpec as P
 
 norm_eps = 1e-06
@@ -155,6 +159,503 @@
     return combined.astype(jnp.bfloat16)
 
 
+MESH = pl.DeviceIdType.MESH
+
+
+def remote(source, target, send_sem, recv_sem, device):
+    return pltpu.make_async_remote_copy(
+        src_ref=source,
+        dst_ref=target,
+        send_sem=send_sem,
+        recv_sem=recv_sem,
+        device_id=device,
+        device_id_type=MESH,
+    )
+
+
+def greet(devices):
+    barrier = pltpu.get_barrier_semaphore()
+    for device in devices:
+        pl.semaphore_signal(barrier, inc=1, device_id=device, device_id_type=MESH)
+    pl.semaphore_wait(barrier, len(devices))
+
+
+def front_kernel(
+    n_ep,
+    n_tp,
+    slots_ref,
+    select_ref,
+    route_weights_ref,
+    query_ref,
+    key_ref,
+    value_ref,
+    cos_ref,
+    sin_ref,
+    gate_hbm,
+    up_hbm,
+    down_hbm,
+    expert_ref,
+    all_ref,
+    packed,
+    gathered,
+    gate_vmem,
+    up_vmem,
+    down_vmem,
+    hidden,
+    partial,
+    arrived,
+    summed,
+    returned,
+    weight_sem,
+    local_sem,
+    disp_send,
+    disp_recv,
+    gath_send,
+    gath_recv,
+    part_send,
+    part_recv,
+    ret_send,
+    ret_recv,
+    qkv_send,
+    qkv_recv,
+    pair_send,
+    pair_recv,
+):
+    ep = lax.axis_index("ep")
+    tp = lax.axis_index("tp")
+    n_z = n_ep // 2
+    z, core = ep // 2, lax.rem(ep, 2)
+    capacity, width = slots_ref.shape[1:]
+    rows = n_ep * capacity
+    head_width = packed.shape[2] // 3
+    half = head_width // 2
+    weights = [
+        pltpu.make_async_copy(gate_hbm, gate_vmem, weight_sem.at[0]),
+        pltpu.make_async_copy(up_hbm, up_vmem, weight_sem.at[1]),
+        pltpu.make_async_copy(down_hbm, down_vmem, weight_sem.at[2]),
+    ]
+    for copy in weights:
+        copy.start()
+    greet(
+        [{"ep": lax.rem(ep + d, n_ep)} for d in range(1, n_ep)]
+        + [{"tp": lax.rem(tp + d, n_tp)} for d in range(1, n_tp)]
+    )
+    mine = tp * n_ep + ep
+    dispatch = [pltpu.make_async_copy(slots_ref.at[ep], gathered.at[mine], local_sem.at[0])]
+    for d in range(1, n_ep):
+        target = lax.rem(ep + d, n_ep)
+        dispatch.append(
+            remote(
+                slots_ref.at[target],
+                gathered.at[mine],
+                disp_send.at[d],
+                disp_recv.at[d],
+                {"ep": target},
+            )
+        )
+    for copy in dispatch:
+        copy.start()
+
+    for head in range(n_z):
+        for index, ref in ((0, query_ref), (1, key_ref)):
+            for m in range(2):
+                at = head * head_width + m * half
+                entry = ref[:, at : at + half].astype(jnp.float32)
+                turned = entry * cos_ref[...] + pltpu.roll(entry, half // 2, 1) * sin_ref[...]
+                to = index * head_width + m * half
+                packed[head, :, to : to + half] = turned.astype(jnp.bfloat16)
+        packed[head, :, 2 * head_width :] = value_ref[
+            :, head * head_width : (head + 1) * head_width
+        ]
+    exchange = [pltpu.make_async_copy(packed.at[z], all_ref.at[ep], local_sem.at[1])]
+    for d in range(1, n_z):
+        target = lax.rem(z + d, n_z)
+        exchange.append(
+            remote(
+                packed.at[target],
+                all_ref.at[ep],
+                qkv_send.at[d],
+                qkv_recv.at[d],
+                {"ep": 2 * target + core},
+            )
+        )
+    for copy in exchange:
+        copy.start()
+
+    spread = []
+    for d in range(n_ep):
+        source = lax.rem(ep + n_ep - d, n_ep)
+        if d == 0:
+            dispatch[0].wait()
+        else:
+            dispatch[d].wait_recv()
+        slot = gathered.at[tp * n_ep + source]
+        for t in range(1, n_tp):
+            copy = remote(
+                slot,
+                slot,
+                gath_send.at[d * n_tp + t],
+                gath_recv.at[d * n_tp + t],
+                {"tp": lax.rem(tp + t, n_tp)},
+            )
+            copy.start()
+            spread.append(copy)
+    for copy in spread:
+        copy.wait_recv()
+    weights[0].wait()
+    weights[1].wait()
+    tile = 256
+
+    def hidden_tile(j, carry):
+        columns = pl.ds(pl.multiple_of(j * tile, tile), tile)
+        gate = jnp.zeros((rows, tile), jnp.float32)
+        up = jnp.zeros((rows, tile), jnp.float32)
+        for i in range(n_tp):
+            block = gathered[i * n_ep : (i + 1) * n_ep].reshape(rows, width)
+            gate += jnp.dot(
+                block,
+                gate_vmem[0, i * width : (i + 1) * width, columns],
+                preferred_element_type=jnp.float32,
+            )
+            up += jnp.dot(
+                block,
+                up_vmem[0, i * width : (i + 1) * width, columns],
+                preferred_element_type=jnp.float32,
+            )
+        hidden[:, columns] = (gate / (1.0 + jnp.exp(-gate)) * up).astype(jnp.bfloat16)
+        return carry
+
+    lax.fori_loop(0, hidden.shape[1] // tile, hidden_tile, 0)
+    weights[2].wait()
+    scatter = []
+    for d in list(range(1, n_tp)) + [0]:
+        target = lax.rem(tp + d, n_tp)
+        columns = pl.ds(pl.multiple_of(target * width, width), width)
+        partial[d] = jnp.dot(
+            hidden[...], down_vmem[0, :, columns], preferred_element_type=jnp.float32
+        ).astype(jnp.bfloat16)
+        if d:
+            copy = remote(
+                partial.at[d], arrived.at[d], part_send.at[d], part_recv.at[d], {"tp": target}
+            )
+            copy.start()
+            scatter.append(copy)
+    total = partial[0].astype(jnp.float32)
+    for d in range(1, n_tp):
+        scatter[d - 1].wait_recv()
+        total += arrived[d].astype(jnp.float32)
+    summed[...] = total.astype(jnp.bfloat16).reshape(n_ep, capacity, width)
+    back = [pltpu.make_async_copy(summed.at[ep], returned.at[ep], local_sem.at[2])]
+    for d in range(1, n_ep):
+        target = lax.rem(ep + d, n_ep)
+        back.append(
+            remote(
+                summed.at[target],
+                returned.at[ep],
+                ret_send.at[d],
+                ret_recv.at[d],
+                {"ep": target},
+            )
+        )
+    for copy in back:
+        copy.start()
+
+    pairs = []
+    for d in range(n_z):
+        source = 2 * lax.rem(z + n_z - d, n_z) + core
+        if d == 0:
+            exchange[0].wait()
+        else:
+            exchange[d].wait_recv()
+        part = all_ref.at[source, :, pl.ds(head_width, 2 * head_width)]
+        copy = remote(part, part, pair_send.at[d], pair_recv.at[d], {"ep": ep + 1 - 2 * core})
+        copy.start()
+        pairs.append(copy)
+
+    back[0].wait()
+    for copy in back[1:]:
+        copy.wait_recv()
+    flat = returned[...].reshape(rows, width)
+    result = jnp.zeros(expert_ref.shape, jnp.float32)
+    for k in range(select_ref.shape[0]):
+        picked = jnp.dot(select_ref[k], flat, preferred_element_type=jnp.float32)
+        result += route_weights_ref[:, k : k + 1] * picked
+    expert_ref[...] = result.astype(expert_ref.dtype)
+    for copy in pairs:
+        copy.wait_recv()
+    for copy in dispatch[1:] + exchange[1:] + spread + scatter + back[1:] + pairs:
+        copy.wait_send()
+
+
+def back_kernel(
+    n_ep,
+    n_tp,
+    all_ref,
+    lambda_ref,
+    gain_ref,
+    weight_hbm,
+    mixed_ref,
+    weight_vmem,
+    heads,
+    landed,
+    partial,
+    arrived,
+    weight_sem,
+    head_send,
+    head_recv,
+    part_send,
+    part_recv,
+):
+    ep = lax.axis_index("ep")
+    tp = lax.axis_index("tp")
+    n_z = n_ep // 2
+    z, core = ep // 2, lax.rem(ep, 2)
+    row_count = all_ref.shape[1]
+    value_width = gain_ref.shape[1]
+    half = value_width // 2
+    width = mixed_ref.shape[1]
+    weight = pltpu.make_async_copy(weight_hbm, weight_vmem, weight_sem)
+    weight.start()
+    greet(
+        [{"ep": 2 * lax.rem(z + d, n_z) + core} for d in range(1, n_z)]
+        + [{"tp": lax.rem(tp + d, n_tp)} for d in range(1, n_tp)]
+    )
+    scale = half ** (-0.5)
+    pair_rows = 2 * row_count
+    row = lax.broadcasted_iota(jnp.int32, (row_count, pair_rows), 0) + core * row_count
+    causal = lax.broadcasted_iota(jnp.int32, (row_count, pair_rows), 1) <= row
+
+    def sender(block):
+        return remote(
+            heads.at[block],
+            landed.at[z],
+            head_send.at[block],
+            head_recv.at[z],
+            {"ep": 2 * block + core},
+        )
+
+    def keeper(block):
+        return pltpu.make_async_copy(heads.at[block], landed.at[block], head_recv.at[block])
+
+    for block in range(n_z - 1, -1, -1):
+        maps = []
+        for m in range(2):
+            query = all_ref[2 * block + core, :, m * half : (m + 1) * half]
+            pieces = []
+            for pair in range(block + 1):
+                at = value_width + m * half
+                keys = all_ref[2 * pair : 2 * pair + 2, :, at : at + half].reshape(pair_rows, half)
+                scores = lax.dot_general(
+                    query, keys, (((1,), (1,)), ((), ())), preferred_element_type=jnp.float32
+                )
+                scores = scores * scale
+                if pair == block:
+                    scores = jnp.where(causal, scores, -1e30)
+                pieces.append(scores)
+            peak = functools.reduce(
+                jnp.maximum, [jnp.max(piece, axis=1, keepdims=True) for piece in pieces]
+            )
+            total = jnp.zeros((row_count, 1), jnp.float32)
+            outcome = jnp.zeros((row_count, value_width), jnp.float32)
+            for pair in range(block + 1):
+                expd = jnp.exp(pieces[pair] - peak)
+                total += jnp.sum(expd, axis=1, keepdims=True)
+                values = all_ref[2 * pair : 2 * pair + 2, :, 2 * value_width :].reshape(
+                    pair_rows, value_width
+                )
+                outcome += jnp.dot(
+                    expd.astype(jnp.bfloat16), values, preferred_element_type=jnp.float32
+                )
+            maps.append(outcome / total)
+        difference = maps[0] - lambda_ref[...] * maps[1]
+        mean = jnp.mean(difference * difference, axis=1, keepdims=True)
+        heads[block] = (difference * lax.rsqrt(mean + norm_eps) * gain_ref[...]).astype(
+            jnp.bfloat16
+        )
+
+        @pl.when(z == block)
+        def _():
+            keeper(block).start()
+
+        @pl.when(z != block)
+        def _():
+            sender(block).start()
+
+    for block in range(n_z):
+        keeper(block).wait()
+    weight.wait()
+    scatter = []
+    for d in list(range(1, n_tp)) + [0]:
+        target = lax.rem(tp + d, n_tp)
+        columns = pl.ds(pl.multiple_of(target * width, width), width)
+        product = jnp.zeros((row_count, width), jnp.float32)
+        for h in range(n_z):
+            product += jnp.dot(
+                landed[h],
+                weight_vmem[h * value_width : (h + 1) * value_width, columns],
+                preferred_element_type=jnp.float32,
+            )
+        partial[d] = product.astype(jnp.bfloat16)
+        if d:
+            copy = remote(
+                partial.at[d], arrived.at[d], part_send.at[d], part_recv.at[d], {"tp": target}
+            )
+            copy.start()
+            scatter.append(copy)
+    total = partial[0].astype(jnp.float32)
+    for d in range(1, n_tp):
+        scatter[d - 1].wait_recv()
+        total += arrived[d].astype(jnp.float32)
+    mixed_ref[...] = total.astype(jnp.bfloat16)
+    for copy in scatter:
+        copy.wait_send()
+    for block in range(n_z):
+
+        @pl.when(z != block)
+        def _():
+            sender(block).wait_send()
+
+
+def fused(
+    query_maps,
+    key_maps,
+    value_rows,
+    head_lambda,
+    head_gain,
+    out_weight,
+    expert_rows,
+    expert_gain,
+    routes,
+    route_weights,
+    gate_weight,
+    up_weight,
+    down_weight,
+):
+    n_ep = lax.axis_size("ep")
+    n_tp = lax.axis_size("tp")
+    n_z = n_ep // 2
+    ep = lax.axis_index("ep")
+    tp = lax.axis_index("tp")
+    row_count = query_maps.shape[0]
+    head_width = query_maps.shape[1] // n_z
+    head_dim = head_width // 2
+    token_count, model_width = expert_rows.shape
+    pick_count = routes.shape[1]
+    capacity = 3 * token_count * pick_count // (2 * n_ep)
+    width = model_width // n_tp
+    hidden_width = gate_weight.shape[2]
+    slot_rows = n_ep * capacity
+
+    positions = ep * row_count + jnp.arange(row_count, dtype=jnp.int32)
+    half_dim = head_dim // 2
+    inverse = rope_base ** (-2.0 * jnp.arange(half_dim, dtype=jnp.float32) / head_dim)
+    angles = positions.astype(jnp.float32)[:, None] * inverse[None, :]
+    cosine, sine = jnp.cos(angles), jnp.sin(angles)
+    cos_table = jnp.concatenate([cosine, cosine], axis=1)
+    sin_table = jnp.concatenate([-sine, sine], axis=1)
+
+    inputs = expert_rows.astype(jnp.float32)
+    inverse_norm = lax.rsqrt(jnp.mean(inputs * inputs, axis=-1, keepdims=True) + norm_eps)
+    part_rows = lax.dynamic_slice_in_dim(expert_rows, tp * width, width, 1).astype(jnp.float32)
+    part_gain = lax.dynamic_slice_in_dim(expert_gain, tp * width, width, 0)
+    normed = (part_rows * inverse_norm * part_gain).astype(jnp.bfloat16)
+    picks = jnp.arange(token_count * pick_count, dtype=jnp.int32)
+    expert_ids = routes.reshape(-1)
+    earlier = (expert_ids[:, None] == expert_ids[None, :]) & (picks[None, :] < picks[:, None])
+    slot_index = jnp.sum(earlier.astype(jnp.int32), axis=1)
+    place = (expert_ids * capacity + slot_index).reshape(token_count, pick_count).T
+    select = place[:, :, None] == jnp.arange(slot_rows, dtype=jnp.int32)[None, None, :]
+    chosen = jnp.any(select, axis=0).astype(jnp.bfloat16)
+    slots = lax.dot_general(
+        chosen, normed, (((0,), (0,)), ((), ())), preferred_element_type=jnp.float32
+    ).astype(jnp.bfloat16)
+    slots = slots.reshape(n_ep, capacity, width)
+
+    vmem = pl.BlockSpec(memory_space=pltpu.VMEM)
+    hbm = pl.BlockSpec(memory_space=pl.ANY)
+    dma = pltpu.SemaphoreType.DMA
+    bf16 = jnp.bfloat16
+    expert_out, everything = pl.pallas_call(
+        functools.partial(front_kernel, n_ep, n_tp),
+        out_shape=(
+            jax.ShapeDtypeStruct((token_count, width), bf16),
+            jax.ShapeDtypeStruct((n_ep, row_count, 3 * head_width), bf16),
+        ),
+        in_specs=[vmem] * 8 + [hbm] * 3,
+        out_specs=(vmem, vmem),
+        scratch_shapes=[
+            pltpu.VMEM((n_z, row_count, 3 * head_width), bf16),
+            pltpu.VMEM((n_tp * n_ep, capacity, width), bf16),
+            pltpu.VMEM(gate_weight.shape, bf16),
+            pltpu.VMEM(up_weight.shape, bf16),
+            pltpu.VMEM(down_weight.shape, bf16),
+            pltpu.VMEM((slot_rows, hidden_width), bf16),
+            pltpu.VMEM((n_tp, slot_rows, width), bf16),
+            pltpu.VMEM((n_tp, slot_rows, width), bf16),
+            pltpu.VMEM((n_ep, capacity, width), bf16),
+            pltpu.VMEM((n_ep, capacity, width), bf16),
+            dma((3,)),
+            dma((3,)),
+            dma((n_ep,)),
+            dma((n_ep,)),
+            dma((n_ep * n_tp,)),
+            dma((n_ep * n_tp,)),
+            dma((n_tp,)),
+            dma((n_tp,)),
+            dma((n_ep,)),
+            dma((n_ep,)),
+            dma((n_z,)),
+            dma((n_z,)),
+            dma((n_z,)),
+            dma((n_z,)),
+        ],
+        compiler_params=pltpu.CompilerParams(
+            collective_id=0, has_side_effects=True, vmem_limit_bytes=56 * 1024 * 1024
+        ),
+        name="front",
+    )(
+        slots,
+        select.astype(bf16),
+        route_weights,
+        query_maps,
+        key_maps,
+        value_rows,
+        cos_table,
+        sin_table,
+        gate_weight,
+        up_weight,
+        down_weight,
+    )
+    mixed = pl.pallas_call(
+        functools.partial(back_kernel, n_ep, n_tp),
+        out_shape=jax.ShapeDtypeStruct((row_count, width), bf16),
+        in_specs=[vmem] * 3 + [hbm],
+        out_specs=vmem,
+        scratch_shapes=[
+            pltpu.VMEM(out_weight.shape, bf16),
+            pltpu.VMEM((n_z, row_count, head_width), bf16),
+            pltpu.VMEM((n_z, row_count, head_width), bf16),
+            pltpu.VMEM((n_tp, row_count, width), bf16),
+            pltpu.VMEM((n_tp, row_count, width), bf16),
+            dma,
+            dma((n_z,)),
+            dma((n_z,)),
+            dma((n_tp,)),
+            dma((n_tp,)),
+        ],
+        compiler_params=pltpu.CompilerParams(
+            collective_id=1, has_side_effects=True, vmem_limit_bytes=56 * 1024 * 1024
+        ),
+        name="back",
+    )(
+        everything,
+        lax.dynamic_slice_in_dim(head_lambda, ep // 2, 1, 0).reshape(1, 1),
+        head_gain.reshape(1, head_width),
+        out_weight,
+    )
+    return (mixed, expert_out)
+
+
 def on_device(
     query_maps,
     key_maps,
@@ -170,6 +671,29 @@
     up_weight,
     down_weight,
 ):
+    n_ep = lax.axis_size("ep")
+    head_count = head_lambda.shape[0]
+    capacity = 3 * expert_rows.shape[0] * routes.shape[1] // (2 * n_ep)
+    if (
+        2 * head_count == n_ep
+        and capacity % 16 == 0
+        and value_rows.shape[1] == query_maps.shape[1] == 256 * head_count
+    ):
+        return fused(
+            query_maps,
+            key_maps,
+            value_rows,
+            head_lambda,
+            head_gain,
+            out_weight,
+            expert_rows,
+            expert_gain,
+            routes,
+            route_weights,
+            gate_weight,
+            up_weight,
+            down_weight,
+        )
     mixed = mixer_half(query_maps, key_maps, value_rows, head_lambda, head_gain, out_weight)
     expert_out = expert_half(
         expert_rows, expert_gain, routes, route_weights, gate_weight, up_weight, down_weight

time: 217 us -> 124 us (0.57)
  Pallas kernels: 0 us -> 110 us
  blocking collectives: 63.6 us -> 0 us
  waiting for transfers between devices: 39.2 us -> 0 us
  local copies, waits for them, and re-layouts: 39.1 us -> 6.9 us
  matrix products: 33.2 us -> 2 us
  between operations: 15.8 us -> 0.71 us
  other arithmetic: 18.9 us -> 4.3 us
  starting transfers between devices: 5.1 us -> 0 us
    pallas_call x0 -> x2, Pallas kernels: none -> 110 us  [the longest x1 70.2 us: fused(): pl.pallas_call(functools.partial(front_kernel, n_ep, n_tp), out_shape=(ja...]
    all_to_all x1 -> x0, blocking collectives: 63.6 us -> none  [expert_half(): lax.all_to_all(empty.at[expert_ids, slot_index].set(normed[source_row]),...]
    dot_general x8 -> x1, matrix products: 33.2 us -> 2 us  [fused(): lax.dot_general(chosen, normed, (((0,), (0,)), ((), ())), preferred_eleme...]
    scatter x1 -> x0, local copies, waits for them, and re-layouts: 23.1 us -> none  [expert_half(): empty.at[expert_ids, slot_index].set(normed[source_row])]
    all_gather x2 -> x0, waiting for transfers between devices: 18.8 us -> none  [the longest x1 18.7 us: mixer_half(): piece_v = lax.all_gather(value_rows, 'ep', axis=0, tiled=True)]
    all_to_all x1 -> x0, waiting for transfers between devices: 12.4 us -> none  [expert_half(): lax.all_to_all(summed, 'ep', split_axis=0, concat_axis=0, tiled=True)]
    reduce_sum x6 -> x2, other arithmetic: 13 us -> 1.41 us  [the longest x1 1.23 us: fused(): jnp.mean(inputs * inputs, axis=-1, keepdims=True) + norm_eps]
    reduce_scatter x2 -> x0, waiting for transfers between devices: 7.95 us -> none  [the longest x1 7.92 us: mixer_half(): lax.psum_scatter(partial_value.astype(jnp.bfloat16), 'tp', scatter_dimens...]
  transfers between devices with their start and end apart: 5 -> 0, of which waited for: 3 -> 0; matrix products, arithmetic and copies ran while one was open for 40% -> 0% of each run, Pallas kernels for 0% -> 0%
where the time goes in v1:
time: 124 us
  Pallas kernels  110 us (89%)
  local copies, waits for them, and re-layouts  6.9 us (6%)
  other arithmetic  4.3 us (3%)
  matrix products  2 us (2%)
    pallas_call x1, Pallas kernels, fused(): pl.pallas_call(functools.partial(front_kernel, n_ep, n_tp), out_shape=(ja...  70.2 us
    pallas_call x1, Pallas kernels, fused(): pl.pallas_call(functools.partial(back_kernel, n_ep, n_tp), out_shape=jax....  40 us
    unnamed x6, local copies, waits for them, and re-layouts  4.53 us

profile of v1, /device:TPU:0, one launch (start us, length us, event | category | flops | bytes accessed | tf_op | source)
XLA Modules:
  0.0 124.1 jit_solution(4554997188992531768)
XLA Ops:
  0.6 1.3 %dynamic_slice.11 = f32[1]{0:T(128)} dynamic-slice(f32[4]{0:T(128)} %param.16, s32[]{:T(128)S(6)} %select_n.14), dynamic_slice_sizes={1} | dynamic-slice | bytes 12 | tf_op jit(solution)/shard_map/dynamic_slice | solution.py:652
  1.9 1.2 multiply_reduce_fusion
  3.2 0.8 dynamic_slice.10
  3.9 1.4 %copy.28.route_weights_ref = f32[128,2]{1,0:T(8,128)} copy(f32[128,2]{0,1:T(2,128)} %param.22) | data formatting | bytes 2048 | tf_op args[9]
  5.4 0.8 copy.26
  6.1 0.1 eq.28
  6.3 0.2 convert_reduce_fusion
  6.5 0.1 reduce_sum.21
  6.6 0.1 copy.27
  6.7 0.7 add_bitcast_fusion
  7.4 0.8 fusion
  8.2 2.0 %convolution_convert_fusion = bf16[384,512]{1,0:T(8,128)(2,1)} fusion(pred[128,384]{1,0:T(8,128)(4,1)S(1)} %get-tuple-element.10, f32[512]{0:T(512)S(1)} %dynamic_slice.10, f32[128]{0:T(128)S(1)} %add_rsqrt_fusion, bf16[128,2048]{1,0:T(8,128)(2,1)} %param.19, s32[]{:T(128)S(6)} %select_n.12), kind=kOutput, calls=%fused_computation | convolution fusion | flops 50790400 | bytes 576004 | tf_op jit(solution)/shard_map/dot_general | solution.py:569
  10.2 0.5 fusion.6
  10.7 0.8 pad_maximum_fusion
  11.6 70.2 %front.1 = (bf16[128,512]{1,0:T(8,128)(2,1)}, bf16[8,256,768]{2,1,0:T(8,128)(2,1)}) custom-call(bf16[8,48,512]{2,1,0:T(8,128)(2,1)} %bitcast.6, bf16[2,128,384]{2,1,0:T(8,128)(2,1)} %get-tuple-element.9.select_ref, f32[128,2]{1,0:T(8,128)} %copy.28.route_weights_ref, bf16[256,1024]{1,0:T(8,128)(2,1)} %query_ref.1, bf16[256,1024]{1,0:T(8,128)(2,1)} %key_ref.1, ...), custom_call_target="tpu_custom_call" | custom-call | tf_op jit(solution)/shard_map/front/pallas_call | solution.py:578
  81.7 0.0 copy-start
  81.8 40.0 %back.1 = bf16[256,512]{1,0:T(8,128)(2,1)} custom-call(bf16[8,256,768]{2,1,0:T(8,128)(2,1)} %get-tuple-element.4.all_ref, f32[1,1]{1,0:T(1,128)} %bitcast.2.lambda_ref, f32[1,256]{1,0:T(1,128)} %bitcast.7, bf16[1024,2048]{1,0:T(8,128)(2,1)} %weight_hbm.1), custom_call_target="tpu_custom_call" | custom-call | tf_op jit(solution)/shard_map/back/pallas_call | solution.py:629
  121.7 1.7 %copy.31 = bf16[256,512]{1,0:T(8,128)(2,1)} copy(bf16[256,512]{1,0:T(8,128)(2,1)} %back.1) | data formatting | bytes 524288
  123.4 0.0 copy-done
  123.4 0.7 copy.32
  (3 shorter events, 0.0 us)
Async XLA Ops:
  81.7 41.7 %copy-start = (bf16[128,512]{1,0:T(8,128)(2,1)S(1)}, bf16[128,512]{1,0:T(8,128)(2,1)}, u32[]{:S(2)}) copy-start(bf16[128,512]{1,0:T(8,128)(2,1)} %get-tuple-element.16) | copy-start | bytes 393220

commit v2 on v1

--- a/solution.py
+++ b/solution.py
@@ -173,28 +173,27 @@
     )
 
 
-def greet(devices):
-    barrier = pltpu.get_barrier_semaphore()
-    for device in devices:
-        pl.semaphore_signal(barrier, inc=1, device_id=device, device_id_type=MESH)
-    pl.semaphore_wait(barrier, len(devices))
-
-
-def front_kernel(
+def layer_kernel(
     n_ep,
     n_tp,
-    slots_ref,
-    select_ref,
+    rows_ref,
+    norm_gain_ref,
+    routes_ref,
     route_weights_ref,
     query_ref,
     key_ref,
     value_ref,
     cos_ref,
     sin_ref,
+    lambda_ref,
+    gain_ref,
     gate_hbm,
     up_hbm,
     down_hbm,
+    weight_hbm,
     expert_ref,
+    mixed_ref,
+    slots_ref,
     all_ref,
     packed,
     gathered,
@@ -206,6 +205,11 @@
     arrived,
     summed,
     returned,
+    weight_vmem,
+    heads,
+    landed,
+    mixed_partial,
+    mixed_arrived,
     weight_sem,
     local_sem,
     disp_send,
@@ -220,6 +224,10 @@
     qkv_recv,
     pair_send,
     pair_recv,
+    head_send,
+    head_recv,
+    mixed_send,
+    mixed_recv,
 ):
     ep = lax.axis_index("ep")
     tp = lax.axis_index("tp")
@@ -233,13 +241,50 @@
         pltpu.make_async_copy(gate_hbm, gate_vmem, weight_sem.at[0]),
         pltpu.make_async_copy(up_hbm, up_vmem, weight_sem.at[1]),
         pltpu.make_async_copy(down_hbm, down_vmem, weight_sem.at[2]),
+        pltpu.make_async_copy(weight_hbm, weight_vmem, weight_sem.at[3]),
     ]
     for copy in weights:
         copy.start()
-    greet(
-        [{"ep": lax.rem(ep + d, n_ep)} for d in range(1, n_ep)]
-        + [{"tp": lax.rem(tp + d, n_tp)} for d in range(1, n_tp)]
-    )
+    peers = [{"ep": lax.rem(ep + d, n_ep)} for d in range(1, n_ep)]
+    peers += [{"tp": lax.rem(tp + d, n_tp)} for d in range(1, n_tp)]
+    barrier = pltpu.get_barrier_semaphore()
+    for device in peers:
+        pl.semaphore_signal(barrier, inc=1, device_id=device, device_id_type=MESH)
+
+    token_count = rows_ref.shape[0]
+    picks = routes_ref.shape[0]
+    entries = rows_ref[...].astype(jnp.float32)
+    inverse_norm = lax.rsqrt(jnp.mean(entries * entries, axis=1, keepdims=True) + norm_eps)
+    own = pl.ds(pl.multiple_of(tp * width, width), width)
+    normed = rows_ref[:, own].astype(jnp.float32) * inverse_norm * norm_gain_ref[:, own]
+    normed = normed.astype(jnp.bfloat16)
+    named_rows = -(-n_ep // 16) * 16
+    label = lax.broadcasted_iota(jnp.int32, (named_rows, token_count), 0)
+    named = [
+        jnp.where(label == routes_ref[k : k + 1, :], 1.0, 0.0).astype(jnp.float32)
+        for k in range(picks)
+    ]
+    before = lax.broadcasted_iota(jnp.int32, (token_count, token_count), 0)
+    after = lax.broadcasted_iota(jnp.int32, (token_count, token_count), 1)
+    earlier = jnp.dot(
+        sum(named).astype(jnp.bfloat16),
+        jnp.where(before < after, 1.0, 0.0).astype(jnp.bfloat16),
+        preferred_element_type=jnp.float32,
+    )
+    slot_of = lax.broadcasted_iota(jnp.int32, (rows, token_count), 0)
+    select = []
+    for k in range(picks):
+        rank = jnp.sum(named[k] * earlier, axis=0, keepdims=True).astype(jnp.int32)
+        place = routes_ref[k : k + 1, :] * capacity + rank
+        select.append(jnp.where(slot_of == place, 1.0, 0.0).astype(jnp.float32))
+    slots_ref[...] = (
+        jnp.dot(
+            sum(select).astype(jnp.bfloat16), normed, preferred_element_type=jnp.float32
+        )
+        .astype(jnp.bfloat16)
+        .reshape(n_ep, capacity, width)
+    )
+    pl.semaphore_wait(barrier, len(peers))
     mine = tp * n_ep + ep
     dispatch = [pltpu.make_async_copy(slots_ref.at[ep], gathered.at[mine], local_sem.at[0])]
     for d in range(1, n_ep):
@@ -340,26 +385,6 @@
             )
             copy.start()
             scatter.append(copy)
-    total = partial[0].astype(jnp.float32)
-    for d in range(1, n_tp):
-        scatter[d - 1].wait_recv()
-        total += arrived[d].astype(jnp.float32)
-    summed[...] = total.astype(jnp.bfloat16).reshape(n_ep, capacity, width)
-    back = [pltpu.make_async_copy(summed.at[ep], returned.at[ep], local_sem.at[2])]
-    for d in range(1, n_ep):
-        target = lax.rem(ep + d, n_ep)
-        back.append(
-            remote(
-                summed.at[target],
-                returned.at[ep],
-                ret_send.at[d],
-                ret_recv.at[d],
-                {"ep": target},
-            )
-        )
-    for copy in back:
-        copy.start()
-
     pairs = []
     for d in range(n_z):
         source = 2 * lax.rem(z + n_z - d, n_z) + core
@@ -371,54 +396,15 @@
         copy = remote(part, part, pair_send.at[d], pair_recv.at[d], {"ep": ep + 1 - 2 * core})
         copy.start()
         pairs.append(copy)
-
-    back[0].wait()
-    for copy in back[1:]:
-        copy.wait_recv()
-    flat = returned[...].reshape(rows, width)
-    result = jnp.zeros(expert_ref.shape, jnp.float32)
-    for k in range(select_ref.shape[0]):
-        picked = jnp.dot(select_ref[k], flat, preferred_element_type=jnp.float32)
-        result += route_weights_ref[:, k : k + 1] * picked
-    expert_ref[...] = result.astype(expert_ref.dtype)
     for copy in pairs:
         copy.wait_recv()
-    for copy in dispatch[1:] + exchange[1:] + spread + scatter + back[1:] + pairs:
-        copy.wait_send()
-
-
-def back_kernel(
-    n_ep,
-    n_tp,
-    all_ref,
-    lambda_ref,
-    gain_ref,
-    weight_hbm,
-    mixed_ref,
-    weight_vmem,
-    heads,
-    landed,
-    partial,
-    arrived,
-    weight_sem,
-    head_send,
-    head_recv,
-    part_send,
-    part_recv,
-):
-    ep = lax.axis_index("ep")
-    tp = lax.axis_index("tp")
-    n_z = n_ep // 2
-    z, core = ep // 2, lax.rem(ep, 2)
+
     row_count = all_ref.shape[1]
-    value_width = gain_ref.shape[1]
-    half = value_width // 2
-    width = mixed_ref.shape[1]
-    weight = pltpu.make_async_copy(weight_hbm, weight_vmem, weight_sem)
-    weight.start()
-    greet(
-        [{"ep": 2 * lax.rem(z + d, n_z) + core} for d in range(1, n_z)]
-        + [{"tp": lax.rem(tp + d, n_tp)} for d in range(1, n_tp)]
+    value_width = head_width
+    head_weight = jnp.sum(
+        jnp.where(lax.broadcasted_iota(jnp.int32, lambda_ref.shape, 1) == z, lambda_ref[...], 0.0),
+        axis=1,
+        keepdims=True,
     )
     scale = half ** (-0.5)
     pair_rows = 2 * row_count
@@ -437,7 +423,7 @@
     def keeper(block):
         return pltpu.make_async_copy(heads.at[block], landed.at[block], head_recv.at[block])
 
-    for block in range(n_z - 1, -1, -1):
+    def attend(block):
         maps = []
         for m in range(2):
             query = all_ref[2 * block + core, :, m * half : (m + 1) * half]
@@ -467,7 +453,7 @@
                     expd.astype(jnp.bfloat16), values, preferred_element_type=jnp.float32
                 )
             maps.append(outcome / total)
-        difference = maps[0] - lambda_ref[...] * maps[1]
+        difference = maps[0] - head_weight * maps[1]
         mean = jnp.mean(difference * difference, axis=1, keepdims=True)
         heads[block] = (difference * lax.rsqrt(mean + norm_eps) * gain_ref[...]).astype(
             jnp.bfloat16
@@ -481,10 +467,50 @@
         def _():
             sender(block).start()
 
+    order = [n_z - 1] + [0] * (n_z > 1) + list(range(n_z - 2, 0, -1))
+    for block in order[:2]:
+        attend(block)
+    total = partial[0].astype(jnp.float32)
+    for d in range(1, n_tp):
+        scatter[d - 1].wait_recv()
+        total += arrived[d].astype(jnp.float32)
+    summed[...] = total.astype(jnp.bfloat16).reshape(n_ep, capacity, width)
+    back = [pltpu.make_async_copy(summed.at[ep], returned.at[ep], local_sem.at[2])]
+    for d in range(1, n_ep):
+        target = lax.rem(ep + d, n_ep)
+        back.append(
+            remote(
+                summed.at[target],
+                returned.at[ep],
+                ret_send.at[d],
+                ret_recv.at[d],
+                {"ep": target},
+            )
+        )
+    for copy in back:
+        copy.start()
+
+    for block in order[2:]:
+        attend(block)
+    back[0].wait()
+    for copy in back[1:]:
+        copy.wait_recv()
+    flat = returned[...].reshape(rows, width)
+    result = jnp.zeros(expert_ref.shape, jnp.float32)
+    for k in range(picks):
+        picked = lax.dot_general(
+            select[k].astype(jnp.bfloat16),
+            flat,
+            (((0,), (0,)), ((), ())),
+            preferred_element_type=jnp.float32,
+        )
+        spread_out = jnp.where(before == after, route_weights_ref[k : k + 1, :], 0.0)
+        result += jnp.sum(spread_out, axis=1, keepdims=True) * picked
+    expert_ref[...] = result.astype(expert_ref.dtype)
     for block in range(n_z):
         keeper(block).wait()
-    weight.wait()
-    scatter = []
+    weights[3].wait()
+    mixed_scatter = []
     for d in list(range(1, n_tp)) + [0]:
         target = lax.rem(tp + d, n_tp)
         columns = pl.ds(pl.multiple_of(target * width, width), width)
@@ -495,25 +521,27 @@
                 weight_vmem[h * value_width : (h + 1) * value_width, columns],
                 preferred_element_type=jnp.float32,
             )
-        partial[d] = product.astype(jnp.bfloat16)
+        mixed_partial[d] = product.astype(jnp.bfloat16)
         if d:
             copy = remote(
-                partial.at[d], arrived.at[d], part_send.at[d], part_recv.at[d], {"tp": target}
+                mixed_partial.at[d], mixed_arrived.at[d], mixed_send.at[d], mixed_recv.at[d], {"tp": target}
             )
             copy.start()
-            scatter.append(copy)
-    total = partial[0].astype(jnp.float32)
+            mixed_scatter.append(copy)
+    total = mixed_partial[0].astype(jnp.float32)
     for d in range(1, n_tp):
-        scatter[d - 1].wait_recv()
-        total += arrived[d].astype(jnp.float32)
+        mixed_scatter[d - 1].wait_recv()
+        total += mixed_arrived[d].astype(jnp.float32)
     mixed_ref[...] = total.astype(jnp.bfloat16)
-    for copy in scatter:
+    for copy in mixed_scatter:
         copy.wait_send()
     for block in range(n_z):
 
         @pl.when(z != block)
         def _():
             sender(block).wait_send()
+    for copy in dispatch[1:] + exchange[1:] + spread + scatter + back[1:] + pairs:
+        copy.wait_send()
 
 
 def fused(
@@ -535,13 +563,11 @@
     n_tp = lax.axis_size("tp")
     n_z = n_ep // 2
     ep = lax.axis_index("ep")
-    tp = lax.axis_index("tp")
     row_count = query_maps.shape[0]
     head_width = query_maps.shape[1] // n_z
     head_dim = head_width // 2
     token_count, model_width = expert_rows.shape
-    pick_count = routes.shape[1]
-    capacity = 3 * token_count * pick_count // (2 * n_ep)
+    capacity = 3 * token_count * routes.shape[1] // (2 * n_ep)
     width = model_width // n_tp
     hidden_width = gate_weight.shape[2]
     slot_rows = n_ep * capacity
@@ -554,36 +580,21 @@
     cos_table = jnp.concatenate([cosine, cosine], axis=1)
     sin_table = jnp.concatenate([-sine, sine], axis=1)
 
-    inputs = expert_rows.astype(jnp.float32)
-    inverse_norm = lax.rsqrt(jnp.mean(inputs * inputs, axis=-1, keepdims=True) + norm_eps)
-    part_rows = lax.dynamic_slice_in_dim(expert_rows, tp * width, width, 1).astype(jnp.float32)
-    part_gain = lax.dynamic_slice_in_dim(expert_gain, tp * width, width, 0)
-    normed = (part_rows * inverse_norm * part_gain).astype(jnp.bfloat16)
-    picks = jnp.arange(token_count * pick_count, dtype=jnp.int32)
-    expert_ids = routes.reshape(-1)
-    earlier = (expert_ids[:, None] == expert_ids[None, :]) & (picks[None, :] < picks[:, None])
-    slot_index = jnp.sum(earlier.astype(jnp.int32), axis=1)
-    place = (expert_ids * capacity + slot_index).reshape(token_count, pick_count).T
-    select = place[:, :, None] == jnp.arange(slot_rows, dtype=jnp.int32)[None, None, :]
-    chosen = jnp.any(select, axis=0).astype(jnp.bfloat16)
-    slots = lax.dot_general(
-        chosen, normed, (((0,), (0,)), ((), ())), preferred_element_type=jnp.float32
-    ).astype(jnp.bfloat16)
-    slots = slots.reshape(n_ep, capacity, width)
-
     vmem = pl.BlockSpec(memory_space=pltpu.VMEM)
     hbm = pl.BlockSpec(memory_space=pl.ANY)
     dma = pltpu.SemaphoreType.DMA
     bf16 = jnp.bfloat16
-    expert_out, everything = pl.pallas_call(
-        functools.partial(front_kernel, n_ep, n_tp),
+    expert_out, mixed = pl.pallas_call(
+        functools.partial(layer_kernel, n_ep, n_tp),
         out_shape=(
             jax.ShapeDtypeStruct((token_count, width), bf16),
-            jax.ShapeDtypeStruct((n_ep, row_count, 3 * head_width), bf16),
+            jax.ShapeDtypeStruct((row_count, width), bf16),
         ),
-        in_specs=[vmem] * 8 + [hbm] * 3,
+        in_specs=[vmem] * 11 + [hbm] * 4,
         out_specs=(vmem, vmem),
         scratch_shapes=[
+            pltpu.VMEM((n_ep, capacity, width), bf16),
+            pltpu.VMEM((n_ep, row_count, 3 * head_width), bf16),
             pltpu.VMEM((n_z, row_count, 3 * head_width), bf16),
             pltpu.VMEM((n_tp * n_ep, capacity, width), bf16),
             pltpu.VMEM(gate_weight.shape, bf16),
@@ -594,7 +605,12 @@
             pltpu.VMEM((n_tp, slot_rows, width), bf16),
             pltpu.VMEM((n_ep, capacity, width), bf16),
             pltpu.VMEM((n_ep, capacity, width), bf16),
-            dma((3,)),
+            pltpu.VMEM(out_weight.shape, bf16),
+            pltpu.VMEM((n_z, row_count, head_width), bf16),
+            pltpu.VMEM((n_z, row_count, head_width), bf16),
+            pltpu.VMEM((n_tp, row_count, width), bf16),
+            pltpu.VMEM((n_tp, row_count, width), bf16),
+            dma((4,)),
             dma((3,)),
             dma((n_ep,)),
             dma((n_ep,)),
@@ -608,49 +624,30 @@
             dma((n_z,)),
             dma((n_z,)),
             dma((n_z,)),
-        ],
-        compiler_params=pltpu.CompilerParams(
-            collective_id=0, has_side_effects=True, vmem_limit_bytes=56 * 1024 * 1024
-        ),
-        name="front",
-    )(
-        slots,
-        select.astype(bf16),
-        route_weights,
-        query_maps,
-        key_maps,
-        value_rows,
-        cos_table,
-        sin_table,
-        gate_weight,
-        up_weight,
-        down_weight,
-    )
-    mixed = pl.pallas_call(
-        functools.partial(back_kernel, n_ep, n_tp),
-        out_shape=jax.ShapeDtypeStruct((row_count, width), bf16),
-        in_specs=[vmem] * 3 + [hbm],
-        out_specs=vmem,
-        scratch_shapes=[
-            pltpu.VMEM(out_weight.shape, bf16),
-            pltpu.VMEM((n_z, row_count, head_width), bf16),
-            pltpu.VMEM((n_z, row_count, head_width), bf16),
-            pltpu.VMEM((n_tp, row_count, width), bf16),
-            pltpu.VMEM((n_tp, row_count, width), bf16),
-            dma,
             dma((n_z,)),
             dma((n_z,)),
             dma((n_tp,)),
             dma((n_tp,)),
         ],
         compiler_params=pltpu.CompilerParams(
-            collective_id=1, has_side_effects=True, vmem_limit_bytes=56 * 1024 * 1024
+            collective_id=0, has_side_effects=True, vmem_limit_bytes=60 * 1024 * 1024
         ),
-        name="back",
+        name="layer",
     )(
-        everything,
-        lax.dynamic_slice_in_dim(head_lambda, ep // 2, 1, 0).reshape(1, 1),
+        expert_rows,
+        expert_gain.reshape(1, model_width),
+        routes.T,
+        route_weights.T,
+        query_maps,
+        key_maps,
+        value_rows,
+        cos_table,
+        sin_table,
+        head_lambda.reshape(1, n_z),
         head_gain.reshape(1, head_width),
+        gate_weight,
+        up_weight,
+        down_weight,
         out_weight,
     )
     return (mixed, expert_out)

time: 124 us -> 93 us (0.75)
  the two profiles are of different devices: /device:TPU:0 before, /device:TPU:9 now
where the time goes in v2:
time: 93 us; the launch traced here: 92.8 us
  Pallas kernels  87.5 us (94%)
  local copies, waits for them, and re-layouts  3.24 us (3%)
  other arithmetic  1.39 us (1%)
    pallas_call x1, Pallas kernels, fused(): pl.pallas_call(functools.partial(layer_kernel, n_ep, n_tp), out_shape=(ja...  87.5 us
    unnamed x2, local copies, waits for them, and re-layouts  3.24 us

profile of v2, /device:TPU:9, one launch (start us, length us, event | category | flops | bytes accessed | tf_op | source)
XLA Modules:
  0.0 92.8 jit_solution(5810024201643977500)
XLA Ops:
  0.7 0.5 fusion
  1.2 0.8 pad_maximum_fusion
  2.0 87.5 %layer.1 = (bf16[128,512]{1,0:T(8,128)(2,1)}, bf16[256,512]{1,0:T(8,128)(2,1)}) custom-call(bf16[128,2048]{1,0:T(8,128)(2,1)} %rows_ref.1, f32[1,2048]{1,0:T(1,128)} %bitcast.5, s32[2,128]{1,0:T(2,128)} %bitcast.6, f32[2,128]{1,0:T(2,128)} %bitcast.7, bf16[256,1024]{1,0:T(8,128)(2,1)} %query_ref.1, bf16[256,1024]{1,0:T(8,128)(2,1)} %key_ref.1, ...), custom_call_target="tpu_custom_call" | custom-call | tf_op jit(solution)/shard_map/layer/pallas_call | solution.py:587
  89.6 1.7 %copy.17 = bf16[256,512]{1,0:T(8,128)(2,1)} copy(bf16[256,512]{1,0:T(8,128)(2,1)} %get-tuple-element.13) | data formatting | bytes 524288
  91.3 1.6 %copy.18 = bf16[128,512]{1,0:T(8,128)(2,1)} copy(bf16[128,512]{1,0:T(8,128)(2,1)} %get-tuple-element.14) | data formatting | bytes 262144
  (2 shorter events, 0.0 us)
